TPU v7x, 512 devices: a 4x2x32 block of a 4x8x32 slice. The times are simulated.
512 devices in a mesh: grp: 2 (over y), sp: 32 (over z), tp: 8 (over x, core).
Axes of the slice: x: 4, y: 2, z: 32, core: 2. Of those that a mesh axis runs over, the one named last changes fastest.
The devices are a block of a 4x8x32 slice.
Arguments:
- stream: bfloat16 [49152, 4096], P(('grp', 'sp'), 'tp'), parts along dimension 0, may hold values from -400 to 400
- in_weight: bfloat16 [2, 1024, 4096], P(None, 'sp', 'tp'), may hold values from -0.09375 to 0.09375
- out_weight: bfloat16 [2, 1024, 4096], P(None, 'sp', 'tp'), may hold values from -0.1875 to 0.1875
- group_mix: bfloat16 [2, 4, 256, 256], replicated, may hold values from -0.375 to 0.375
- pool_gain: float32 [2, 1024], replicated, may hold values from 0.1 to 1.9
- norm_gain: float32 [2, 4096], P(None, 'tp'), may hold values from 0.1 to 1.9
- norm_shift: float32 [2, 4096], P(None, 'tp'), may hold values from -3 to 3
Outputs:
- refined: bfloat16 [49152, 4096], P(('grp', 'sp'), 'tp'), parts along dimension 0
There are 2 independent parts, one for each index of `grp`. A program takes and returns all parts, laid end to end along the dimension named above; an argument that names none is the same for every part. Nothing has to cross between parts.
All inputs are finite; a program needn't handle non-finite values.
Results may differ from a plain program's by a relative error of at most 0.015.
Values may be sent and summed in bfloat16 or wider, within the bound.
A program may use at most 64 MiB of HBM per device.

v0:
```python
import jax
import jax.numpy as jnp
from jax import lax
from jax.sharding import PartitionSpec as P

D = 4096
POOL = 1024
GROUPS = 4
GROUP_WIDTH = 256
LAYERS = 2


epsilon = 1e-05


def passed_along(block, axis, distance):
    devices = range(lax.axis_size(axis))
    route = [(i - distance, i) for i in devices if i - distance in devices]
    return lax.ppermute(block, axis, route)


def sent_together(arrays, axis, dim, along):
    widths = [a.shape[along] for a in arrays]
    both = jnp.concatenate(arrays, axis=along)
    whole = lax.all_gather(both, axis, axis=dim, tiled=True)
    return tuple(jnp.split(whole, [sum(widths[:k]) for k in range(1, len(widths))], axis=along))


def split_up(x, dim, devices):
    shape = x.shape
    pieces = x.reshape(*shape[:dim], devices, shape[dim] // devices, *shape[dim + 1 :])
    return jnp.moveaxis(pieces, dim, 0)


def sent_and_summed(x, axis, dim):
    pieces = split_up(x, dim, lax.axis_size(axis))
    arrived = lax.all_to_all(pieces, axis, split_axis=0, concat_axis=0, tiled=True)
    return arrived.astype(jnp.float32).sum(axis=0)


def copy_for_each(x, axis):
    copies = jnp.broadcast_to(x, (lax.axis_size(axis), *x.shape))
    return lax.all_to_all(copies, axis, split_axis=0, concat_axis=0, tiled=True)


def in_order(pieces, dim):
    pieces = jnp.moveaxis(pieces, 0, dim)
    shape = pieces.shape
    return pieces.reshape(*shape[:dim], shape[dim] * shape[dim + 1], *shape[dim + 2 :])


def gathered_copies(x, axis, dim):
    pieces = copy_for_each(x, axis)
    return in_order(pieces, dim)


def taken_together(x, axis):
    everything = copy_for_each(x, axis)
    return jnp.sum(everything, axis=0)


def in_one(arrays, axis):
    ravelled, at, gathered = (jnp.concatenate([a.reshape(-1) for a in arrays]), 0, [])
    total = taken_together(ravelled, axis)
    for a in arrays:
        gathered.append(total[at : at + a.size].reshape(a.shape))
        at += a.size
    return tuple(gathered)


def pooled_windows(hidden, chan_start, tok_start):
    reach = 2**GROUPS - 1
    length = hidden.shape[1]
    channels = hidden.shape[0]
    earlier = passed_along(hidden[:, length - reach :], "sp", 1)
    extended = jnp.concatenate([earlier, hidden], axis=1).astype(jnp.float32)
    group_ids = ((chan_start + jnp.arange(channels, dtype=jnp.int32)) // GROUP_WIDTH)[:, None]
    running = extended
    window_sums = jnp.zeros((channels, length), jnp.float32)
    for octave in range(GROUPS):
        offset = 2**octave
        running = running[:, offset:] + running[:, : running.shape[1] - offset]
        window_sums = jnp.where(
            group_ids == octave, running[:, running.shape[1] - length :], window_sums
        )
    positions = (tok_start + jnp.arange(length, dtype=jnp.int32) + 1).astype(jnp.float32)
    widths = jnp.exp2((group_ids + 1).astype(jnp.float32))
    counts = jnp.minimum(positions[None, :], widths)
    return (window_sums / counts - hidden.astype(jnp.float32)).astype(jnp.bfloat16)


def per_device(stream, in_weight, out_weight, group_mix, pool_gain, norm_gain, norm_shift):
    tok_rows = stream.shape[0]
    tok_start = lax.axis_index("sp") * tok_rows
    share = POOL // lax.axis_size("tp")
    chan_start = lax.axis_index("tp") * share
    alpha = (2.0 * LAYERS) ** 0.25
    contract_rows = (((0,), (0,)), ((), ()))
    contract_cols = (((1,), (1,)), ((), ()))
    every_in, every_out = sent_together((in_weight, out_weight), "sp", 1, 0)
    current = stream
    for layer_index in range(LAYERS):
        whole_in = every_in[layer_index]
        hidden_share = sent_and_summed(
            lax.dot_general(
                whole_in, current, contract_cols, preferred_element_type=jnp.float32
            ).astype(jnp.bfloat16),
            "tp",
            0,
        ).astype(jnp.bfloat16)
        pooled_part = pooled_windows(hidden_share, chan_start, tok_start)
        pooled = gathered_copies(pooled_part, "tp", 0)
        grouped = pooled.reshape(GROUPS, GROUP_WIDTH, tok_rows)
        mixed = jnp.einsum(
            "gio,git->got", group_mix[layer_index], grouped, preferred_element_type=jnp.float32
        )
        gains = pool_gain[layer_index].reshape(GROUPS, GROUP_WIDTH, 1)
        scaled = (mixed * gains).astype(jnp.bfloat16).reshape(POOL, tok_rows)
        branch = lax.dot_general(
            scaled, every_out[layer_index], contract_rows, preferred_element_type=jnp.float32
        )
        summed = alpha * current.astype(jnp.float32) + branch
        row_sum, row_squares = in_one(
            (jnp.sum(summed, axis=1), jnp.sum(summed * summed, axis=1)), "tp"
        )
        row_mean = row_sum / D
        row_var = row_squares / D - row_mean * row_mean
        normed = (summed - row_mean[:, None]) * lax.rsqrt(row_var + epsilon)[:, None]
        current = (
            normed * norm_gain[layer_index][None, :] + norm_shift[layer_index][None, :]
        ).astype(jnp.bfloat16)
    return current


def solution(mesh):
    in_specs = (
        P(("grp", "sp"), "tp"),
        P(None, "sp", "tp"),
        P(None, "sp", "tp"),
        P(),
        P(),
        P(None, "tp"),
        P(None, "tp"),
    )
    out_specs = P(("grp", "sp"), "tp")
    return jax.shard_map(
        per_device, mesh=mesh, in_specs=in_specs, out_specs=out_specs, check_vma=False
    )
```

profile of v0, /device:TPU:33, one launch (start us, length us, event | category | flops | bytes accessed | tf_op | source)
XLA Modules:
  0.0 331.2 jit_solution(1252397504181705562)
XLA Ops:
  6.5 0.0 all-gather.2.cloned.1.call-start
  6.6 1.5 pad_maximum_fusion
  8.1 0.1 all-gather.2.cloned.1.call-update
  8.2 147.8 %all-gather.2.cloned.1.call-done = bf16[4,1024,512]{2,1,0:T(8,128)(2,1)} async-done(((bf16[4,32,512]{2,1,0:T(8,128)(2,1)}), bf16[4,1024,512]{2,1,0:T(8,128)(2,1)}) %all-gather.2.cloned.1.call-update) | async-done | bytes 4194320 | tf_op jit(solution)/shard_map/all_gather | solution.py:25
  155.9 3.6 %convolution_convert_fusion.1 = bf16[1024,768]{1,0:T(8,128)(2,1)} fusion(bf16[768,512]{1,0:T(8,128)(2,1)} %param.7, bf16[4,1024,512]{2,1,0:T(8,128)(2,1)} %all-gather.2.cloned.1.call-done), kind=kOutput, calls=%fused_computation.3 | convolution fusion | flops 806092800 | bytes 3407872 | tf_op jit(solution)/shard_map/dot_general | solution.py:105
  159.6 24.8 %all-to-all-start = ((bf16[8,128,768]{2,1,0:T(8,128)(2,1)}), bf16[8,128,768]{2,1,0:T(8,128)(2,1)S(1)}, u32[]{:S(2)}, u32[]{:S(2)}) async-start(bf16[8,128,768]{2,1,0:T(8,128)(2,1)} %bitcast.1), calls=%async_computation | async-start | bytes 3145728 | tf_op jit(solution)/shard_map/all_to_all | solution.py:37
  184.4 20.5 %all-to-all-done = bf16[8,128,768]{2,1,0:T(8,128)(2,1)S(1)} async-done(((bf16[8,128,768]{2,1,0:T(8,128)(2,1)}), bf16[8,128,768]{2,1,0:T(8,128)(2,1)S(1)}, u32[]{:S(2)}, u32[]{:S(2)}) %all-to-all-start) | async-done | bytes 1572896 | tf_op jit(solution)/shard_map/all_to_all | solution.py:37
  204.9 0.2 reduce_sum.78
  205.2 0.1 slice.159
  205.3 2.2 collective-permute-start
  207.4 1.0 collective-permute-done
  208.4 0.1 maximum_convert_fusion
  208.6 0.2 slice_add_fusion.5
  208.8 0.2 slice_add_fusion.4
  208.9 0.2 slice_add_fusion.3
  209.1 0.5 fusion.5
  209.7 1.3 broadcast_in_dim.59
  210.9 0.0 copy-start.1
  210.9 5.5 %all-to-all-start.1 = ((bf16[8,128,768]{2,1,0:T(8,128)(2,1)}), bf16[8,128,768]{2,1,0:T(8,128)(2,1)S(1)}, u32[]{:S(2)}, u32[]{:S(2)}) async-start(bf16[8,128,768]{2,1,0:T(8,128)(2,1)} %broadcast_in_dim.59), calls=%async_computation.1 | async-start | bytes 3145728 | tf_op jit(solution)/shard_map/all_to_all | solution.py:43
  216.4 0.0 copy-done.1
  216.4 0.0 copy-start.3
  216.4 0.0 copy-start.4
  216.4 0.0 copy-start
  216.4 1.2 copy.16
  217.6 0.0 copy-done.3
  217.6 0.0 copy-done.4
  217.6 19.4 %all-to-all-done.1 = bf16[8,128,768]{2,1,0:T(8,128)(2,1)S(1)} async-done(((bf16[8,128,768]{2,1,0:T(8,128)(2,1)}), bf16[8,128,768]{2,1,0:T(8,128)(2,1)S(1)}, u32[]{:S(2)}, u32[]{:S(2)}) %all-to-all-start.1) | async-done | bytes 1572896 | tf_op jit(solution)/shard_map/all_to_all | solution.py:43
  237.1 0.0 copy-done
  237.1 0.0 copy-start.2
  237.1 0.7 multiply_convert_fusion.1
  237.7 0.5 copy-done.2
  238.2 0.0 copy-start.5
  238.2 2.4 fusion.21
  240.6 0.0 copy-start.6
  240.7 0.7 broadcast_in_dim.60
  241.4 4.2 %all-to-all-start.2 = ((f32[8,1,1536]{2,1,0:T(1,128)}), f32[8,1,1536]{2,1,0:T(1,128)S(1)}, u32[]{:S(2)}, u32[]{:S(2)}) async-start(f32[8,1,1536]{2,1,0:T(1,128)} %broadcast_in_dim.60), calls=%async_computation.2 | async-start | bytes 98304 | tf_op jit(solution)/shard_map/all_to_all | solution.py:43
  245.6 0.0 copy-done.5
  245.6 4.8 %all-to-all-done.2 = f32[8,1,1536]{2,1,0:T(1,128)S(1)} async-done(((f32[8,1,1536]{2,1,0:T(1,128)}), f32[8,1,1536]{2,1,0:T(1,128)S(1)}, u32[]{:S(2)}, u32[]{:S(2)}) %all-to-all-start.2) | async-done | bytes 49184 | tf_op jit(solution)/shard_map/all_to_all | solution.py:43
  250.5 2.4 convolution_convert_fusion
  252.9 0.0 copy-done.6
  252.9 23.8 %all_to_all.32 = bf16[8,128,768]{2,1,0:T(8,128)(2,1)S(1)} all-to-all(bf16[8,128,768]{2,1,0:T(8,128)(2,1)S(1)} %bitcast.47), channel_id=1, replica_groups=mesh['grp'=2,'sp'=32,'tp'=8] {'tp'}, dimensions={0} | all-to-all | bytes 3145728 | tf_op jit(solution)/shard_map/all_to_all | solution.py:37
  276.8 0.2 reduce_sum.82
  277.0 0.1 slice.174
  277.1 4.0 %collective-permute-start.1 = (bf16[128,15]{1,0:T(8,128)(2,1)S(1)}, bf16[128,15]{1,0:T(8,128)(2,1)S(1)}, u32[]{:S(2)}, u32[]{:S(2)}) collective-permute-start(bf16[128,15]{1,0:T(8,128)(2,1)S(1)} %slice.174), channel_id=1, source_target_pairs={{0,8},{8,16},{16,24},{24,32},{32,40},{40,48},{48,56},{56,64},{64,7... | collective-permute-start | bytes 11528 | tf_op jit(solution)/shard_map/ppermute | solution.py:19
  281.0 1.0 collective-permute-done.1
  282.0 0.1 maximum_convert_fusion.1
  282.2 0.2 slice_add_fusion.2
  282.4 0.2 slice_add_fusion.1
  282.6 0.2 slice_add_fusion
  282.7 0.5 fusion.7
  283.3 1.3 broadcast_in_dim.61
  284.6 5.4 %all-to-all-start.4 = ((bf16[8,128,768]{2,1,0:T(8,128)(2,1)}), bf16[8,128,768]{2,1,0:T(8,128)(2,1)S(1)}, u32[]{:S(2)}, u32[]{:S(2)}) async-start(bf16[8,128,768]{2,1,0:T(8,128)(2,1)} %broadcast_in_dim.61), calls=%async_computation.4 | async-start | bytes 3145728 | tf_op jit(solution)/shard_map/all_to_all | solution.py:43
  290.0 20.7 %all-to-all-done.4 = bf16[8,128,768]{2,1,0:T(8,128)(2,1)S(1)} async-done(((bf16[8,128,768]{2,1,0:T(8,128)(2,1)}), bf16[8,128,768]{2,1,0:T(8,128)(2,1)S(1)}, u32[]{:S(2)}, u32[]{:S(2)}) %all-to-all-start.4) | async-done | bytes 1572896 | tf_op jit(solution)/shard_map/all_to_all | solution.py:43
  310.6 0.0 copy-start.7
  310.6 0.6 multiply_convert_fusion
  311.3 0.8 copy-done.7
  312.0 2.6 fusion.20
  314.7 8.2 %all_to_all.33 = f32[8,1,1536]{2,1,0:T(1,128)S(1)} all-to-all(f32[8,1,1536]{2,1,0:T(1,128)S(1)} %broadcast_in_dim.62), channel_id=1, replica_groups=mesh['grp'=2,'sp'=32,'tp'=8] {'tp'}, dimensions={0} | all-to-all | bytes 98304 | tf_op jit(solution)/shard_map/all_to_all | solution.py:43
  322.9 0.3 add_convert_fusion
  323.2 1.2 copy.21
  (16 shorter events, 0.2 us)
Async XLA Ops:
  6.5 149.4 %all-gather.2.cloned.1.call-start = ((), (), s32[]{:S(2)}) async-start(), calls=%async_computation.6 | async-start | bytes 4325376 | tf_op jit(solution)/shard_map/all_gather | solution.py:25
  159.6 45.4 %all-to-all-start = ((bf16[8,128,768]{2,1,0:T(8,128)(2,1)}), bf16[8,128,768]{2,1,0:T(8,128)(2,1)S(1)}, u32[]{:S(2)}, u32[]{:S(2)}) async-start(bf16[8,128,768]{2,1,0:T(8,128)(2,1)} %bitcast.1), calls=%async_computation | async-start | bytes 3145728 | tf_op jit(solution)/shard_map/all_to_all | solution.py:37
  205.3 3.2 collective-permute-start
  210.9 5.5 %copy-start.1 = (bf16[768,512]{1,0:T(8,128)(2,1)S(1)}, bf16[768,512]{1,0:T(8,128)(2,1)}, u32[]{:S(2)}) copy-start(bf16[768,512]{1,0:T(8,128)(2,1)} %param.7) | copy-start | bytes 2359300
  210.9 26.1 %all-to-all-start.1 = ((bf16[8,128,768]{2,1,0:T(8,128)(2,1)}), bf16[8,128,768]{2,1,0:T(8,128)(2,1)S(1)}, u32[]{:S(2)}, u32[]{:S(2)}) async-start(bf16[8,128,768]{2,1,0:T(8,128)(2,1)} %broadcast_in_dim.59), calls=%async_computation.1 | async-start | bytes 3145728 | tf_op jit(solution)/shard_map/all_to_all | solution.py:43
  216.4 1.2 copy-start.3
  216.4 1.2 copy-start.4
  216.4 20.7 %copy-start = (bf16[2,4,256,256]{3,2,1,0:T(8,128)(2,1)S(1)}, bf16[2,4,256,256]{3,2,1,0:T(8,128)(2,1)}, u32[]{:S(2)}) copy-start(bf16[2,4,256,256]{3,2,1,0:T(8,128)(2,1)} %param.10) | copy-start | bytes 3145732
  237.1 1.1 copy-start.2
  238.2 7.4 %copy-start.5 = (f32[2,512]{1,0:T(2,128)S(1)}, f32[2,512]{1,0:T(2,128)}, u32[]{:S(2)}) copy-start(f32[2,512]{1,0:T(2,128)} %param.13) | copy-start | bytes 12292
  240.6 12.3 %copy-start.6 = (f32[768,512]{0,1:T(8,128)}, f32[768,512]{0,1:T(8,128)S(1)}, u32[]{:S(2)}) copy-start(f32[768,512]{0,1:T(8,128)S(1)} %get-tuple-element.19) | copy-start | bytes 4718596
  241.4 9.1 %all-to-all-start.2 = ((f32[8,1,1536]{2,1,0:T(1,128)}), f32[8,1,1536]{2,1,0:T(1,128)S(1)}, u32[]{:S(2)}, u32[]{:S(2)}) async-start(f32[8,1,1536]{2,1,0:T(1,128)} %broadcast_in_dim.60), calls=%async_computation.2 | async-start | bytes 98304 | tf_op jit(solution)/shard_map/all_to_all | solution.py:43
  277.1 5.0 %collective-permute-start.1 = (bf16[128,15]{1,0:T(8,128)(2,1)S(1)}, bf16[128,15]{1,0:T(8,128)(2,1)S(1)}, u32[]{:S(2)}, u32[]{:S(2)}) collective-permute-start(bf16[128,15]{1,0:T(8,128)(2,1)S(1)} %slice.174), channel_id=1, source_target_pairs={{0,8},{8,16},{16,24},{24,32},{32,40},{40,48},{48,56},{56,64},{64,7... | collective-permute-start | bytes 11528 | tf_op jit(solution)/shard_map/ppermute | solution.py:19
  284.6 26.1 %all-to-all-start.4 = ((bf16[8,128,768]{2,1,0:T(8,128)(2,1)}), bf16[8,128,768]{2,1,0:T(8,128)(2,1)S(1)}, u32[]{:S(2)}, u32[]{:S(2)}) async-start(bf16[8,128,768]{2,1,0:T(8,128)(2,1)} %broadcast_in_dim.61), calls=%async_computation.4 | async-start | bytes 3145728 | tf_op jit(solution)/shard_map/all_to_all | solution.py:43
  310.6 1.4 copy-start.7
Sparse Core Ops, SparseCore 0:
  9.4 146.4 all-gather.1
where the time goes:
time: 332 us; the launch traced here: 331 us
  waiting for transfers between devices  215 us (65%)
  starting transfers between devices  46 us (14%)
  blocking collectives  32 us (10%)
  between operations  13.7 us (4%)
  matrix products  12.3 us (4%)
  local copies, waits for them, and re-layouts  7.1 us (2%)
  other arithmetic  4.84 us (1%)
    all_gather x1, waiting for transfers between devices, sent_together(): whole = lax.all_gather(both, axis, axis=dim, tiled=True)  148 us
    all_to_all x3, waiting for transfers between devices, copy_for_each(): return lax.all_to_all(copies, axis, split_axis=0, concat_axis=0, tiled=True)  44.9 us
    all_to_all x1, starting transfers between devices, sent_and_summed(): lax.all_to_all(pieces, axis, split_axis=0, concat_axis=0, tiled=True)  24.8 us
    all_to_all x1, blocking collectives, sent_and_summed(): lax.all_to_all(pieces, axis, split_axis=0, concat_axis=0, tiled=True)  23.8 us
    all_to_all x1, waiting for transfers between devices, sent_and_summed(): lax.all_to_all(pieces, axis, split_axis=0, concat_axis=0, tiled=True)  20.5 us
    all_to_all x3, starting transfers between devices, copy_for_each(): return lax.all_to_all(copies, axis, split_axis=0, concat_axis=0, tiled=True)  15.1 us
    all_to_all x1, blocking collectives, copy_for_each(): return lax.all_to_all(copies, axis, split_axis=0, concat_axis=0, tiled=True)  8.17 us
  transfers between devices with their start and end apart: 7, of which 7 were waited for; matrix products, arithmetic and copies ran while one was open for 0% of the time, Pallas kernels for 0%

commit v1 on v0

v1 whole, which is shorter than its diff:
```python
import functools

import jax
import jax.numpy as jnp
from jax import lax
from jax.experimental import pallas as pl
from jax.experimental.pallas import tpu as pltpu
from jax.sharding import PartitionSpec as P

D = 4096
GROUPS = 4
GROUP_WIDTH = 256
LAYERS = 2
HALF = GROUP_WIDTH // 2
REACH = 16
HALO = LAYERS * REACH
MESH = pl.DeviceIdType.MESH

epsilon = 1e-05


def kernel(
    n_sp,
    n_tp,
    stream_ref,
    in_ref,
    out_w_ref,
    mix_ref,
    gain_ref,
    norm_gain_ref,
    norm_shift_ref,
    out_ref,
    weights,
    cur,
    band,
    part,
    peer,
    own,
    first,
    second_out,
    second,
    gath,
    summed,
    stat_out,
    stat_in,
    ring_send,
    ring_recv,
    halo_sem,
    part_send,
    part_recv,
    first_send,
    first_recv,
    second_send,
    second_recv,
    gath_send,
    gath_recv,
    stat_send,
    stat_recv,
):
    rows = stream_ref.shape[0]
    block = in_ref.shape[1]
    share = (rows + REACH) // 2 - REACH // 2
    taken = share + HALO
    given = share + REACH
    z = lax.axis_index("sp")
    me = lax.axis_index("tp")
    core = lax.rem(me, 2)
    x = me // 2
    mate = me + 1 - 2 * core
    xa = x + 1 - 2 * lax.rem(x, 2)
    xb = GROUPS - 1 - x
    xo = lax.rem(x + 2, GROUPS)
    dev_a = 2 * xa + core
    dev_b = 2 * xb + core
    right = lax.rem(z + 1, n_sp)
    left = lax.rem(z + n_sp - 1, n_sp)
    alpha = (2.0 * LAYERS) ** 0.25

    barrier = pltpu.get_barrier_semaphore()
    for neighbour in (left, right):
        pl.semaphore_signal(barrier, inc=1, device_id={"sp": neighbour}, device_id_type=MESH)
    for step in range(1, n_tp):
        pl.semaphore_signal(
            barrier, inc=1, device_id={"tp": lax.rem(me + step, n_tp)}, device_id_type=MESH
        )
    pl.semaphore_wait(barrier, 2 + n_tp - 1)

    steps = (n_sp // 2, (n_sp - 1) // 2)

    def at(array, owner):
        return weights.at[array, pl.ds(pl.multiple_of(owner * block, block), block)]

    def owner_of(way, distance):
        if way == 0:
            return lax.rem(z - distance + n_sp, n_sp)
        return lax.rem(z + distance, n_sp)

    def ring_copy(way, array, step, src):
        there = at(array, owner_of(way, step - 1))
        return pltpu.make_async_remote_copy(
            src_ref=there if src is None else src,
            dst_ref=there,
            send_sem=ring_send.at[way, array, step - 1],
            recv_sem=ring_recv.at[way, array, step - 1],
            device_id={"sp": right if way == 0 else left},
            device_id_type=MESH,
        )

    def ring_wait(way, array, step):
        here = at(array, owner_of(way, step))
        pltpu.make_async_remote_copy(
            src_ref=here,
            dst_ref=here,
            send_sem=ring_send.at[way, array, step - 1],
            recv_sem=ring_recv.at[way, array, step - 1],
            device_id={"sp": right if way == 0 else left},
            device_id_type=MESH,
        ).wait_recv()

    halo = pltpu.make_async_remote_copy(
        src_ref=stream_ref.at[pl.ds(rows - HALO, HALO)],
        dst_ref=cur.at[pl.ds(0, HALO)],
        send_sem=halo_sem.at[0],
        recv_sem=halo_sem.at[1],
        device_id={"sp": right},
        device_id_type=MESH,
    )
    sources = [in_ref.at[0], out_w_ref.at[0], in_ref.at[1], out_w_ref.at[1]]
    for array, source in enumerate(sources):
        for way in range(2):
            if steps[way] > 0:
                ring_copy(way, array, 1, source).start()
        if array == 0:
            halo.start()
    for array, source in enumerate(sources):
        at(array, z)[...] = source[...]
    cur[pl.ds(HALO, rows), :] = stream_ref[...]

    window = 2 * jnp.where(x == 0, 1, jnp.where(x == 1, 2, jnp.where(x == 2, 4, 8)))
    start = z * rows - HALO + core * share
    r = lax.broadcasted_iota(jnp.int32, (given, taken), 0) + REACH
    j = lax.broadcasted_iota(jnp.int32, (given, taken), 1)
    count = jnp.clip(start + r + 1, 1, window)
    inside = (r - j >= 0) & (r - j < window) & (start + j >= 0)
    entry = jnp.where(inside, 1.0, 0.0) - jnp.where(r == j, count.astype(jnp.float32), 0.0)
    band[...] = entry.astype(jnp.bfloat16)
    column = lax.broadcasted_iota(jnp.int32, (given, 1), 0) + REACH + start + 1
    scale = 1.0 / jnp.clip(column, 1, window).astype(jnp.float32)

    def forward(step, carry):
        for array in range(2 * LAYERS):
            for way in range(2):
                ring_wait(way, array, step)
                ring_copy(way, array, step + 1, None).start()
        return carry

    if steps[1] > 1:
        lax.fori_loop(1, steps[1], forward, 0)
    for array in range(2 * LAYERS):
        for way in range(2):
            if steps[way] > max(steps[1], 1):
                ring_wait(way, array, steps[way] - 1)
                ring_copy(way, array, steps[way], None).start()
    for array in range(2 * LAYERS):
        for way in range(2):
            if steps[way] > 0:
                ring_wait(way, array, steps[way])
    halo.wait_recv()

    sent = []

    def send(src, dst, sems, to, index):
        copy = pltpu.make_async_remote_copy(
            src_ref=src,
            dst_ref=dst,
            send_sem=sems[0].at[index[0]],
            recv_sem=sems[1].at[index[1]],
            device_id={"tp": to},
            device_id_type=MESH,
        )
        copy.start()
        sent.append(copy)

    def arrive(dst, sems, index):
        pltpu.make_async_remote_copy(
            src_ref=dst,
            dst_ref=dst,
            send_sem=sems[0].at[index[0]],
            recv_sem=sems[1].at[index[1]],
            device_id={"tp": mate},
            device_id_type=MESH,
        ).wait_recv()

    contract_cols = (((1,), (1,)), ((), ()))
    contract = (((1,), (0,)), ((), ()))
    mine = pl.multiple_of(core * share, REACH)
    mates = pl.multiple_of((1 - core) * share, REACH)
    rblock = (rows + REACH) // 7
    eye = lax.broadcasted_iota(jnp.int32, (rblock, 128), 0) == lax.broadcasted_iota(
        jnp.int32, (rblock, 128), 1
    )

    for layer in range(LAYERS):
        order = (xo, xa, xb, x)

        def in_weight_of(g):
            return weights[2 * layer, pl.ds(pl.multiple_of(g * GROUP_WIDTH, GROUP_WIDTH), GROUP_WIDTH)]

        for k, g in enumerate(order):
            product = lax.dot_general(
                cur[pl.ds(mates, taken)], in_weight_of(g), contract_cols,
                preferred_element_type=jnp.float32,
            )
            part[layer, k] = product.astype(jnp.bfloat16)
            send(part.at[layer, k], peer.at[layer, k], (part_send, part_recv), mate,
                 ((layer, k), (layer, k)))
        for k, g in enumerate(order):
            product = lax.dot_general(
                cur[pl.ds(mine, taken)], in_weight_of(g), contract_cols,
                preferred_element_type=jnp.float32,
            )
            arrive(peer.at[layer, k], (part_send, part_recv), ((layer, k), (layer, k)))
            total = (product + peer[layer, k].astype(jnp.float32)).astype(jnp.bfloat16)
            own[layer, k, 0] = total[:, :HALF]
            own[layer, k, 1] = total[:, HALF:]
            f = (first_send, first_recv)
            if k == 0:
                send(own.at[layer, 0, 0], first.at[layer, 0, 1], f, dev_a, ((layer, 0, 1), (layer, 0, 1)))
                send(own.at[layer, 0, 1], first.at[layer, 1, 1], f, dev_b, ((layer, 1, 1), (layer, 1, 1)))
            if k == 1:
                send(own.at[layer, 1, 0], first.at[layer, 0, 0], f, dev_a, ((layer, 0, 0), (layer, 0, 0)))
            if k == 2:
                send(own.at[layer, 2, 1], first.at[layer, 1, 0], f, dev_b, ((layer, 1, 0), (layer, 1, 0)))

        f = (first_send, first_recv)
        s = (second_send, second_recv)
        for half, k, to in ((0, 2, dev_b), (1, 1, dev_a)):
            arrive(first.at[layer, half, 1], f, ((layer, half, 1), (layer, half, 1)))
            second_out[layer, half] = (
                own[layer, k, half].astype(jnp.float32) + first[layer, half, 1].astype(jnp.float32)
            ).astype(jnp.bfloat16)
            send(second_out.at[layer, half], second.at[layer, half], s, to, ((layer, half), (layer, half)))
        pieces = []
        for half in range(2):
            arrive(first.at[layer, half, 0], f, ((layer, half, 0), (layer, half, 0)))
            arrive(second.at[layer, half], s, ((layer, half), (layer, half)))
            pieces.append(
                (
                    own[layer, 3, half].astype(jnp.float32)
                    + first[layer, half, 0].astype(jnp.float32)
                    + second[layer, half].astype(jnp.float32)
                ).astype(jnp.bfloat16)
            )
        hidden = jnp.concatenate(pieces, axis=1)
        pooled = lax.dot_general(band[...], hidden, contract, preferred_element_type=jnp.float32)
        pooled = (pooled * scale).astype(jnp.bfloat16)
        mixed = lax.dot_general(pooled, mix_ref[layer, x], contract, preferred_element_type=jnp.float32)
        scaled = (mixed * gain_ref[layer, x]).astype(jnp.bfloat16)
        gath[layer, core, x, 0] = scaled[:, :HALF]
        gath[layer, core, x, 1] = scaled[:, HALF:]

        def pass_on(g, half, to, slot):
            ref = gath.at[layer, core, g, half]
            send(ref, ref, (gath_send, gath_recv), to, ((layer, slot), (layer, core, g, half)))

        def take_in(side, g, half):
            arrive(gath.at[layer, side, g, half], (gath_send, gath_recv),
                   ((layer, 0), (layer, side, g, half)))

        pass_on(x, 0, dev_b, 0)
        pass_on(x, 1, dev_a, 1)
        pass_on(x, 0, dev_a, 2)
        pass_on(x, 1, dev_b, 3)
        pass_on(x, 0, mate, 4)
        pass_on(x, 1, mate, 5)
        take_in(core, xb, 0)
        pass_on(xb, 0, dev_a, 6)
        take_in(core, xa, 1)
        pass_on(xa, 1, dev_b, 7)
        pass_on(xb, 0, mate, 8)
        pass_on(xa, 1, mate, 9)
        take_in(core, xa, 0)
        pass_on(xa, 0, mate, 10)
        take_in(core, xb, 1)
        pass_on(xb, 1, mate, 11)
        take_in(core, xo, 0)
        pass_on(xo, 0, mate, 12)
        take_in(core, xo, 1)
        pass_on(xo, 1, mate, 13)

        def branch_of(side):
            whole = jnp.concatenate(
                [gath[layer, side, g, half] for g in range(GROUPS) for half in range(2)], axis=1
            )
            return lax.dot_general(
                whole, weights[2 * layer + 1], contract, preferred_element_type=jnp.float32
            )

        summed[pl.ds(mine, given), :] = branch_of(core)
        for g in (x, xb, xa, xo):
            for half in range(2):
                take_in(1 - core, g, half)
        summed[pl.ds(mates, given), :] = branch_of(1 - core)

        stat_out[layer] = jnp.zeros((16, 128), jnp.float32)
        for b in range(7):
            here = pl.ds(b * rblock, rblock)
            value = summed[here, :] + alpha * cur[pl.ds(REACH + b * rblock, rblock), :].astype(jnp.float32)
            summed[here, :] = value
            for at_row, quantity in ((b, value), (8 + b, value * value)):
                total = jnp.sum(quantity, axis=1, keepdims=True)
                stat_out[layer, pl.ds(at_row, 1), :] = jnp.sum(
                    jnp.where(eye, total, 0.0), axis=0, keepdims=True
                )
        q = (stat_send, stat_recv)
        for step in range(1, n_tp):
            to = lax.rem(me + step, n_tp)
            send(stat_out.at[layer], stat_in.at[layer, me], q, to, ((layer, step), (layer, me)))
        stat_in[layer, me] = stat_out[layer]
        for step in range(1, n_tp):
            other = lax.rem(me + step, n_tp)
            arrive(stat_in.at[layer, other], q, ((layer, step), (layer, other)))
        stats = stat_in[layer, 0]
        for k in range(1, n_tp):
            stats = stats + stat_in[layer, k]
        mean = stats[0:8] / D
        var = stats[8:16] / D - mean * mean
        inverse = lax.rsqrt(var + epsilon)
        norm_gain = norm_gain_ref[pl.ds(layer, 1), :]
        norm_shift = norm_shift_ref[pl.ds(layer, 1), :]
        for b in range(7):
            mean_col = jnp.sum(jnp.where(eye, mean[b : b + 1], 0.0), axis=1, keepdims=True)
            inv_col = jnp.sum(jnp.where(eye, inverse[b : b + 1], 0.0), axis=1, keepdims=True)
            value = summed[pl.ds(b * rblock, rblock), :]
            value = (value - mean_col) * inv_col * norm_gain + norm_shift
            if layer < LAYERS - 1:
                cur[pl.ds(REACH + b * rblock, rblock), :] = value.astype(jnp.bfloat16)
            elif b == 0:
                out_ref[pl.ds(0, rblock - REACH), :] = value[REACH:].astype(jnp.bfloat16)
            else:
                out_ref[pl.ds(b * rblock - REACH, rblock), :] = value.astype(jnp.bfloat16)

    for copy in sent:
        copy.wait_send()
    halo.wait_send()

    def drain(step, carry):
        for array in range(2 * LAYERS):
            for way in range(2):
                ring_copy(way, array, step, None).wait_send()
        return carry

    if steps[1] > 0:
        lax.fori_loop(1, steps[1] + 1, drain, 0)
    for array in range(2 * LAYERS):
        if steps[0] > steps[1]:
            ring_copy(0, array, steps[0], None).wait_send()


def per_device(n_sp, n_tp, stream, in_weight, out_weight, group_mix, pool_gain, norm_gain, norm_shift):
    rows, cols = stream.shape
    pool = GROUPS * GROUP_WIDTH
    share = (rows + REACH) // 2 - REACH // 2
    taken, given = share + HALO, share + REACH
    bf, f32 = jnp.bfloat16, jnp.float32
    gains = pool_gain.reshape(LAYERS, GROUPS, 1, GROUP_WIDTH)
    steps = max(n_sp // 2, 1)
    dma = pltpu.SemaphoreType.DMA
    return pl.pallas_call(
        functools.partial(kernel, n_sp, n_tp),
        out_shape=jax.ShapeDtypeStruct((rows, cols), bf),
        in_specs=[pl.BlockSpec(memory_space=pltpu.VMEM)] * 7,
        out_specs=pl.BlockSpec(memory_space=pltpu.VMEM),
        scratch_shapes=[
            pltpu.VMEM((2 * LAYERS, pool, cols), bf),
            pltpu.VMEM((rows + HALO, cols), bf),
            pltpu.VMEM((given, taken), bf),
            pltpu.VMEM((LAYERS, GROUPS, taken, GROUP_WIDTH), bf),
            pltpu.VMEM((LAYERS, GROUPS, taken, GROUP_WIDTH), bf),
            pltpu.VMEM((LAYERS, GROUPS, 2, taken, HALF), bf),
            pltpu.VMEM((LAYERS, 2, 2, taken, HALF), bf),
            pltpu.VMEM((LAYERS, 2, taken, HALF), bf),
            pltpu.VMEM((LAYERS, 2, taken, HALF), bf),
            pltpu.VMEM((LAYERS, 2, GROUPS, 2, given, HALF), bf),
            pltpu.VMEM((rows + REACH, cols), f32),
            pltpu.VMEM((LAYERS, 16, 128), f32),
            pltpu.VMEM((LAYERS, n_tp, 16, 128), f32),
            dma((2, 2 * LAYERS, steps)),
            dma((2, 2 * LAYERS, steps)),
            dma((2,)),
            dma((LAYERS, GROUPS)),
            dma((LAYERS, GROUPS)),
            dma((LAYERS, 2, 2)),
            dma((LAYERS, 2, 2)),
            dma((LAYERS, 2)),
            dma((LAYERS, 2)),
            dma((LAYERS, 14)),
            dma((LAYERS, 2, GROUPS, 2)),
            dma((LAYERS, n_tp)),
            dma((LAYERS, n_tp)),
        ],
        compiler_params=pltpu.CompilerParams(
            collective_id=0, has_side_effects=True, vmem_limit_bytes=48 * 1024 * 1024
        ),
    )(stream, in_weight, out_weight, group_mix, gains, norm_gain, norm_shift)


def solution(mesh):
    in_specs = (
        P(("grp", "sp"), "tp"),
        P(None, "sp", "tp"),
        P(None, "sp", "tp"),
        P(),
        P(),
        P(None, "tp"),
        P(None, "tp"),
    )
    out_specs = P(("grp", "sp"), "tp")
    return jax.shard_map(
        functools.partial(per_device, mesh.shape["sp"], mesh.shape["tp"]),
        mesh=mesh, in_specs=in_specs, out_specs=out_specs, check_vma=False,
    )
```

time: 332 us -> 167 us (0.50)
  waiting for transfers between devices: 215 us -> 0 us
  Pallas kernels: 0 us -> 161 us
  starting transfers between devices: 46 us -> 0 us
  blocking collectives: 32 us -> 0 us
  between operations: 13.7 us -> 0.04 us
  matrix products: 12.3 us -> 0 us
  other arithmetic: 4.84 us -> 0 us
    pallas_call x0 -> x1, Pallas kernels: none -> 161 us  [per_device(): pl.pallas_call(functools.partial(kernel, n_sp, n_tp), out_shape=jax.Shape...]
    all_gather x1 -> x0, waiting for transfers between devices: 148 us -> none  [sent_together(): whole = lax.all_gather(both, axis, axis=dim, tiled=True)]
    all_to_all x4 -> x0, waiting for transfers between devices: 65.5 us -> none  [the longest x3 44.9 us: copy_for_each(): return lax.all_to_all(copies, axis, split_axis=0, concat_axis=0, tiled=True)]
    all_to_all x4 -> x0, starting transfers between devices: 39.8 us -> none  [the longest x1 24.8 us: sent_and_summed(): lax.all_to_all(pieces, axis, split_axis=0, concat_axis=0, tiled=True)]
    all_to_all x2 -> x0, blocking collectives: 32 us -> none  [the longest x1 23.8 us: sent_and_summed(): lax.all_to_all(pieces, axis, split_axis=0, concat_axis=0, tiled=True)]
    dot_general x6 -> x0, matrix products: 12.3 us -> none  [the longest x2 6.04 us: per_device(): lax.dot_general(whole_in, current, contract_cols, preferred_element_type=...]
    ppermute x2 -> x0, starting transfers between devices: 6.13 us -> none  [passed_along(): return lax.ppermute(block, axis, route)]
  transfers between devices with their start and end apart: 7 -> 0, of which waited for: 7 -> 0; matrix products, arithmetic and copies ran while one was open for 0% -> 0% of each run, Pallas kernels for 0% -> 0%
where the time goes in v1:
time: 167 us
  Pallas kernels  161 us (96%)
  local copies, waits for them, and re-layouts  5.66 us (3%)
    pallas_call x1, Pallas kernels, per_device(): pl.pallas_call(functools.partial(kernel, n_sp, n_tp), out_shape=jax.Shape...  161 us
    unnamed x13, local copies, waits for them, and re-layouts  4.92 us

profile of v1, /device:TPU:33, one launch (start us, length us, event | category | flops | bytes accessed | tf_op | source)
XLA Modules:
  0.0 166.6 jit_solution(10456117049950350224)
XLA Ops:
  0.0 0.0 copy-start.5
  0.0 0.0 copy-start.4
  0.0 0.7 reshape.3.gain_ref
  0.7 0.0 copy-done.5
  0.8 0.0 copy-done.4
  0.8 0.0 copy-start
  0.8 1.2 copy-done
  2.0 0.0 copy-start.1
  2.0 1.1 copy-done.1
  3.1 0.0 copy-start.2
  3.1 0.8 copy-done.2
  4.0 0.0 copy-start.3
  4.0 0.8 copy-done.3
  4.8 160.9 %shard_map.73 = bf16[768,512]{1,0:T(8,128)(2,1)S(1)} custom-call(bf16[768,512]{1,0:T(8,128)(2,1)S(1)} %copy-done.1, bf16[2,32,512]{2,1,0:T(8,128)(2,1)S(1)} %copy-done.2, bf16[2,32,512]{2,1,0:T(8,128)(2,1)S(1)} %copy-done.3, bf16[2,4,256,256]{3,2,1,0:T(8,128)(2,1)S(1)} %copy-done, f32[2,4,1,256]{3,2,1,0:T(1,128)S(1)} %reshape.3.gain_ref, ...), custom_call_target="tpu_custom_call" | custom-call | tf_op jit(solution)/shard_map/pallas_call | solution.py:369
  165.7 0.9 copy.9
Async XLA Ops:
  0.0 0.8 copy-start.5
  0.0 0.8 copy-start.4
  0.8 1.2 copy-start
  2.0 1.1 copy-start.1
  3.1 0.8 copy-start.2
  4.0 0.8 copy-start.3

commit v2 on v1

--- a/solution.py
+++ b/solution.py
@@ -13,6 +13,7 @@
 LAYERS = 2
 HALF = GROUP_WIDTH // 2
 REACH = 16
+STRIDE = 4
 HALO = LAYERS * REACH
 MESH = pl.DeviceIdType.MESH
 
@@ -22,14 +23,18 @@
 def kernel(
     n_sp,
     n_tp,
-    stream_ref,
-    in_ref,
-    out_w_ref,
+    stream_hbm,
+    in_hbm,
+    out_hbm,
+    mix_hbm,
+    gain_hbm,
+    norm_gain_hbm,
+    norm_shift_hbm,
+    out_ref,
     mix_ref,
     gain_ref,
     norm_gain_ref,
     norm_shift_ref,
-    out_ref,
     weights,
     cur,
     band,
@@ -43,6 +48,7 @@
     summed,
     stat_out,
     stat_in,
+    load_sem,
     ring_send,
     ring_recv,
     halo_sem,
@@ -57,8 +63,8 @@
     stat_send,
     stat_recv,
 ):
-    rows = stream_ref.shape[0]
-    block = in_ref.shape[1]
+    rows = stream_hbm.shape[0]
+    block = in_hbm.shape[1]
     share = (rows + REACH) // 2 - REACH // 2
     taken = share + HALO
     given = share + REACH
@@ -72,69 +78,123 @@
     xo = lax.rem(x + 2, GROUPS)
     dev_a = 2 * xa + core
     dev_b = 2 * xb + core
-    right = lax.rem(z + 1, n_sp)
-    left = lax.rem(z + n_sp - 1, n_sp)
     alpha = (2.0 * LAYERS) ** 0.25
 
+    def load(src, dst, index):
+        copy = pltpu.make_async_copy(src, dst, load_sem.at[index])
+        copy.start()
+        return copy
+
+    own_rows = pl.ds(pl.multiple_of(z * block, block), block)
+    loads = [
+        load(in_hbm.at[0], weights.at[0, own_rows], 0),
+        load(out_hbm.at[0], weights.at[1, own_rows], 1),
+        load(in_hbm.at[1], weights.at[2, own_rows], 2),
+        load(out_hbm.at[1], weights.at[3, own_rows], 3),
+        load(stream_hbm, cur.at[pl.ds(HALO, rows)], 4),
+        load(mix_hbm, mix_ref, 5),
+        load(gain_hbm, gain_ref, 6),
+        load(norm_gain_hbm, norm_gain_ref, 7),
+        load(norm_shift_hbm, norm_shift_ref, 8),
+    ]
+
     barrier = pltpu.get_barrier_semaphore()
-    for neighbour in (left, right):
-        pl.semaphore_signal(barrier, inc=1, device_id={"sp": neighbour}, device_id_type=MESH)
+    for distance in (1, -1, STRIDE, -STRIDE):
+        pl.semaphore_signal(
+            barrier, inc=1, device_id={"sp": lax.rem(z + distance % n_sp, n_sp)}, device_id_type=MESH
+        )
     for step in range(1, n_tp):
         pl.semaphore_signal(
             barrier, inc=1, device_id={"tp": lax.rem(me + step, n_tp)}, device_id_type=MESH
         )
-    pl.semaphore_wait(barrier, 2 + n_tp - 1)
-
-    steps = (n_sp // 2, (n_sp - 1) // 2)
+    pl.semaphore_wait(barrier, 4 + n_tp - 1)
+
+    classes = n_sp // STRIDE
+    main_steps, back_steps = classes // 2, (classes - 1) // 2
 
     def at(array, owner):
         return weights.at[array, pl.ds(pl.multiple_of(owner * block, block), block)]
 
-    def owner_of(way, distance):
-        if way == 0:
-            return lax.rem(z - distance + n_sp, n_sp)
-        return lax.rem(z + distance, n_sp)
-
-    def ring_copy(way, array, step, src):
-        there = at(array, owner_of(way, step - 1))
+    def along(array, distance):
+        sign = 1 if array % 2 == 0 else -1
+        return lax.rem(z + (sign * distance) % n_sp, n_sp)
+
+    def hop(array, kind, index, owner, to):
+        ref = at(array, owner)
         return pltpu.make_async_remote_copy(
-            src_ref=there if src is None else src,
-            dst_ref=there,
-            send_sem=ring_send.at[way, array, step - 1],
-            recv_sem=ring_recv.at[way, array, step - 1],
-            device_id={"sp": right if way == 0 else left},
+            src_ref=ref,
+            dst_ref=ref,
+            send_sem=ring_send.at[array, kind, index],
+            recv_sem=ring_recv.at[array, kind, index],
+            device_id={"sp": to},
             device_id_type=MESH,
         )
 
-    def ring_wait(way, array, step):
-        here = at(array, owner_of(way, step))
-        pltpu.make_async_remote_copy(
-            src_ref=here,
-            dst_ref=here,
-            send_sem=ring_send.at[way, array, step - 1],
-            recv_sem=ring_recv.at[way, array, step - 1],
-            device_id={"sp": right if way == 0 else left},
-            device_id_type=MESH,
-        ).wait_recv()
-
+    sent_hops = []
+
+    def go(array, kind, index, owner, distance):
+        copy = hop(array, kind, index, owner, along(array, distance))
+        copy.start()
+        sent_hops.append(copy)
+
+    def come(array, kind, index, owner):
+        hop(array, kind, index, owner, along(array, 1)).wait_recv()
+
+    def both(k):
+        found = [(k, -STRIDE * k)] if k <= main_steps else []
+        if 0 < k <= back_steps:
+            found.append((classes - k, STRIDE * k))
+        return found
+
+    def stride_stage(array, k):
+        for index, distance in both(k):
+            kind = 0 if distance <= 0 else 1
+            owner = along(array, distance)
+            if k > 0:
+                come(array, kind, k - 1, owner)
+            if (kind == 0) and k < main_steps:
+                go(array, 0, k, owner, STRIDE)
+            if (kind == 1 or k == 0) and k < back_steps:
+                go(array, 1, k, owner, -STRIDE)
+            go(array, 2, index, owner, 1)
+            go(array, 4, index, owner, -1)
+
+    def near_stage(array, k):
+        for index, distance in both(k):
+            owner = along(array, distance - 1)
+            come(array, 2, index, owner)
+            go(array, 3, index, owner, 1)
+
+    def last_stage(array):
+        for k in range(main_steps + 1):
+            for index, distance in both(k):
+                come(array, 3, index, along(array, distance - 2))
+                come(array, 4, index, along(array, distance + 1))
+
+    def stages(arrays):
+        found = []
+        for k in range(1, main_steps + 1):
+            found.append([functools.partial(stride_stage, array, k) for array in arrays])
+            found.append([functools.partial(near_stage, array, k - 1) for array in arrays])
+        found.append([functools.partial(near_stage, array, main_steps) for array in arrays])
+        return found
+
+    for array in range(2):
+        loads[array].wait()
+        stride_stage(array, 0)
+    loads[4].wait()
     halo = pltpu.make_async_remote_copy(
-        src_ref=stream_ref.at[pl.ds(rows - HALO, HALO)],
+        src_ref=cur.at[pl.ds(rows, HALO)],
         dst_ref=cur.at[pl.ds(0, HALO)],
         send_sem=halo_sem.at[0],
         recv_sem=halo_sem.at[1],
-        device_id={"sp": right},
+        device_id={"sp": lax.rem(z + 1, n_sp)},
         device_id_type=MESH,
     )
-    sources = [in_ref.at[0], out_w_ref.at[0], in_ref.at[1], out_w_ref.at[1]]
-    for array, source in enumerate(sources):
-        for way in range(2):
-            if steps[way] > 0:
-                ring_copy(way, array, 1, source).start()
-        if array == 0:
-            halo.start()
-    for array, source in enumerate(sources):
-        at(array, z)[...] = source[...]
-    cur[pl.ds(HALO, rows), :] = stream_ref[...]
+    halo.start()
+    for array in range(2, 4):
+        loads[array].wait()
+        stride_stage(array, 0)
 
     window = 2 * jnp.where(x == 0, 1, jnp.where(x == 1, 2, jnp.where(x == 2, 4, 8)))
     start = z * rows - HALO + core * share
@@ -147,24 +207,20 @@
     column = lax.broadcasted_iota(jnp.int32, (given, 1), 0) + REACH + start + 1
     scale = 1.0 / jnp.clip(column, 1, window).astype(jnp.float32)
 
-    def forward(step, carry):
-        for array in range(2 * LAYERS):
-            for way in range(2):
-                ring_wait(way, array, step)
-                ring_copy(way, array, step + 1, None).start()
-        return carry
-
-    if steps[1] > 1:
-        lax.fori_loop(1, steps[1], forward, 0)
-    for array in range(2 * LAYERS):
-        for way in range(2):
-            if steps[way] > max(steps[1], 1):
-                ring_wait(way, array, steps[way] - 1)
-                ring_copy(way, array, steps[way], None).start()
-    for array in range(2 * LAYERS):
-        for way in range(2):
-            if steps[way] > 0:
-                ring_wait(way, array, steps[way])
+    for stage in stages((0, 1)):
+        for part_of in stage:
+            part_of()
+    later = stages((2, 3))
+
+    def meanwhile(number):
+        for _ in range(number):
+            if later:
+                for part_of in later.pop(0):
+                    part_of()
+
+    for load in loads[5:]:
+        load.wait()
+    last_stage(0)
     halo.wait_recv()
 
     sent = []
@@ -201,6 +257,8 @@
     )
 
     for layer in range(LAYERS):
+        if layer > 0:
+            last_stage(2 * layer)
         order = (xo, xa, xb, x)
 
         def in_weight_of(g):
@@ -234,12 +292,14 @@
 
         f = (first_send, first_recv)
         s = (second_send, second_recv)
+        meanwhile(2)
         for half, k, to in ((0, 2, dev_b), (1, 1, dev_a)):
             arrive(first.at[layer, half, 1], f, ((layer, half, 1), (layer, half, 1)))
             second_out[layer, half] = (
                 own[layer, k, half].astype(jnp.float32) + first[layer, half, 1].astype(jnp.float32)
             ).astype(jnp.bfloat16)
             send(second_out.at[layer, half], second.at[layer, half], s, to, ((layer, half), (layer, half)))
+        meanwhile(2)
         pieces = []
         for half in range(2):
             arrive(first.at[layer, half, 0], f, ((layer, half, 0), (layer, half, 0)))
@@ -255,7 +315,11 @@
         pooled = lax.dot_general(band[...], hidden, contract, preferred_element_type=jnp.float32)
         pooled = (pooled * scale).astype(jnp.bfloat16)
         mixed = lax.dot_general(pooled, mix_ref[layer, x], contract, preferred_element_type=jnp.float32)
-        scaled = (mixed * gain_ref[layer, x]).astype(jnp.bfloat16)
+        gains = jnp.zeros((1, GROUP_WIDTH), jnp.float32)
+        for g in range(GROUPS):
+            of_g = gain_ref[pl.ds(layer, 1), pl.ds(g * GROUP_WIDTH, GROUP_WIDTH)]
+            gains = jnp.where(x == g, of_g, gains)
+        scaled = (mixed * gains).astype(jnp.bfloat16)
         gath[layer, core, x, 0] = scaled[:, :HALF]
         gath[layer, core, x, 1] = scaled[:, HALF:]
 
@@ -273,12 +337,14 @@
         pass_on(x, 1, dev_b, 3)
         pass_on(x, 0, mate, 4)
         pass_on(x, 1, mate, 5)
+        meanwhile(2)
         take_in(core, xb, 0)
         pass_on(xb, 0, dev_a, 6)
         take_in(core, xa, 1)
         pass_on(xa, 1, dev_b, 7)
         pass_on(xb, 0, mate, 8)
         pass_on(xa, 1, mate, 9)
+        meanwhile(2)
         take_in(core, xa, 0)
         pass_on(xa, 0, mate, 10)
         take_in(core, xb, 1)
@@ -296,6 +362,7 @@
                 whole, weights[2 * layer + 1], contract, preferred_element_type=jnp.float32
             )
 
+        last_stage(2 * layer + 1)
         summed[pl.ds(mine, given), :] = branch_of(core)
         for g in (x, xb, xa, xo):
             for half in range(2):
@@ -317,12 +384,15 @@
             to = lax.rem(me + step, n_tp)
             send(stat_out.at[layer], stat_in.at[layer, me], q, to, ((layer, step), (layer, me)))
         stat_in[layer, me] = stat_out[layer]
+        meanwhile(len(later))
         for step in range(1, n_tp):
             other = lax.rem(me + step, n_tp)
             arrive(stat_in.at[layer, other], q, ((layer, step), (layer, other)))
         stats = stat_in[layer, 0]
         for k in range(1, n_tp):
             stats = stats + stat_in[layer, k]
+        if layer == 0:
+            halo.wait_send()
         mean = stats[0:8] / D
         var = stats[8:16] / D - mean * mean
         inverse = lax.rsqrt(var + epsilon)
@@ -340,21 +410,8 @@
             else:
                 out_ref[pl.ds(b * rblock - REACH, rblock), :] = value.astype(jnp.bfloat16)
 
-    for copy in sent:
+    for copy in sent + sent_hops:
         copy.wait_send()
-    halo.wait_send()
-
-    def drain(step, carry):
-        for array in range(2 * LAYERS):
-            for way in range(2):
-                ring_copy(way, array, step, None).wait_send()
-        return carry
-
-    if steps[1] > 0:
-        lax.fori_loop(1, steps[1] + 1, drain, 0)
-    for array in range(2 * LAYERS):
-        if steps[0] > steps[1]:
-            ring_copy(0, array, steps[0], None).wait_send()
 
 
 def per_device(n_sp, n_tp, stream, in_weight, out_weight, group_mix, pool_gain, norm_gain, norm_shift):
@@ -363,15 +420,18 @@
     share = (rows + REACH) // 2 - REACH // 2
     taken, given = share + HALO, share + REACH
     bf, f32 = jnp.bfloat16, jnp.float32
-    gains = pool_gain.reshape(LAYERS, GROUPS, 1, GROUP_WIDTH)
-    steps = max(n_sp // 2, 1)
+    classes = n_sp // STRIDE
     dma = pltpu.SemaphoreType.DMA
     return pl.pallas_call(
         functools.partial(kernel, n_sp, n_tp),
         out_shape=jax.ShapeDtypeStruct((rows, cols), bf),
-        in_specs=[pl.BlockSpec(memory_space=pltpu.VMEM)] * 7,
+        in_specs=[pl.BlockSpec(memory_space=pl.ANY)] * 7,
         out_specs=pl.BlockSpec(memory_space=pltpu.VMEM),
         scratch_shapes=[
+            pltpu.VMEM(group_mix.shape, bf),
+            pltpu.VMEM(pool_gain.shape, f32),
+            pltpu.VMEM(norm_gain.shape, f32),
+            pltpu.VMEM(norm_shift.shape, f32),
             pltpu.VMEM((2 * LAYERS, pool, cols), bf),
             pltpu.VMEM((rows + HALO, cols), bf),
             pltpu.VMEM((given, taken), bf),
@@ -385,8 +445,9 @@
             pltpu.VMEM((rows + REACH, cols), f32),
             pltpu.VMEM((LAYERS, 16, 128), f32),
             pltpu.VMEM((LAYERS, n_tp, 16, 128), f32),
-            dma((2, 2 * LAYERS, steps)),
-            dma((2, 2 * LAYERS, steps)),
+            dma((9,)),
+            dma((2 * LAYERS, 5, classes)),
+            dma((2 * LAYERS, 5, classes)),
             dma((2,)),
             dma((LAYERS, GROUPS)),
             dma((LAYERS, GROUPS)),
@@ -400,9 +461,9 @@
             dma((LAYERS, n_tp)),
         ],
         compiler_params=pltpu.CompilerParams(
-            collective_id=0, has_side_effects=True, vmem_limit_bytes=48 * 1024 * 1024
+            collective_id=0, has_side_effects=True, vmem_limit_bytes=60 * 1024 * 1024
         ),
-    )(stream, in_weight, out_weight, group_mix, gains, norm_gain, norm_shift)
+    )(stream, in_weight, out_weight, group_mix, pool_gain, norm_gain, norm_shift)
 
 
 def solution(mesh):

time: 167 us -> 166 us (level)
  local copies, waits for them, and re-layouts: 5.66 us -> 2.06 us
  Pallas kernels: 161 us -> 163 us
    unnamed x13 -> x1, local copies, waits for them, and re-layouts: 4.92 us -> 2.06 us
    pallas_call x1, Pallas kernels: 161 us -> 163 us  [per_device(): pl.pallas_call(functools.partial(kernel, n_sp, n_tp), out_shape=jax.Shape...]
where the time goes in v2:
time: 166 us
  Pallas kernels  163 us (98%)
  local copies, waits for them, and re-layouts  2.06 us (1%)
    pallas_call x1, Pallas kernels, per_device(): pl.pallas_call(functools.partial(kernel, n_sp, n_tp), out_shape=jax.Shape...  163 us

profile of v2, /device:TPU:33, one launch (start us, length us, event | category | flops | bytes accessed | tf_op | source)
XLA Modules:
  0.0 165.5 jit_solution(14658834229362009357)
XLA Ops:
  0.0 163.4 %shard_map.73 = bf16[768,512]{1,0:T(8,128)(2,1)} custom-call(bf16[768,512]{1,0:T(8,128)(2,1)} %stream_hbm.1, bf16[2,32,512]{2,1,0:T(8,128)(2,1)} %in_hbm.1, bf16[2,32,512]{2,1,0:T(8,128)(2,1)} %out_hbm.1, bf16[2,4,256,256]{3,2,1,0:T(8,128)(2,1)} %mix_hbm.1, f32[2,1024]{1,0:T(2,128)} %gain_hbm.1, f32[2,512]{1,0:T(2,128)} %norm_gain_hbm.1, f32[2,512]{1,0:T(2,128)} %norm_shift_hbm.1), custom_call_target="tpu_custom_call" | custom-call | tf_op jit(solution)/shard_map/pallas_call | solution.py:425
  163.4 2.1 %copy.9 = bf16[768,512]{1,0:T(8,128)(2,1)} copy(bf16[768,512]{1,0:T(8,128)(2,1)} %shard_map.73) | data formatting | bytes 1572864

commit v3 on v2

--- a/solution.py
+++ b/solution.py
@@ -14,6 +14,8 @@
 HALF = GROUP_WIDTH // 2
 REACH = 16
 STRIDE = 4
+LAGS = (0, 0, 10, 10)
+POLLS = (0, 4, 4, 4, 6, 40)
 HALO = LAYERS * REACH
 MESH = pl.DeviceIdType.MESH
 
@@ -51,6 +53,8 @@
     load_sem,
     ring_send,
     ring_recv,
+    pair_send,
+    pair_recv,
     halo_sem,
     part_send,
     part_recv,
@@ -70,6 +74,7 @@
     given = share + REACH
     z = lax.axis_index("sp")
     me = lax.axis_index("tp")
+    part_at = lax.axis_index("grp")
     core = lax.rem(me, 2)
     x = me // 2
     mate = me + 1 - 2 * core
@@ -99,7 +104,8 @@
     ]
 
     barrier = pltpu.get_barrier_semaphore()
-    for distance in (1, -1, STRIDE, -STRIDE):
+    reached = (1, -1, STRIDE, -STRIDE)
+    for distance in reached:
         pl.semaphore_signal(
             barrier, inc=1, device_id={"sp": lax.rem(z + distance % n_sp, n_sp)}, device_id_type=MESH
         )
@@ -107,7 +113,9 @@
         pl.semaphore_signal(
             barrier, inc=1, device_id={"tp": lax.rem(me + step, n_tp)}, device_id_type=MESH
         )
-    pl.semaphore_wait(barrier, 4 + n_tp - 1)
+    beside = part_at + 1 - 2 * lax.rem(part_at, 2)
+    pl.semaphore_signal(barrier, inc=1, device_id={"grp": beside}, device_id_type=MESH)
+    pl.semaphore_wait(barrier, len(reached) + 1 + n_tp - 1)
 
     classes = n_sp // STRIDE
     main_steps, back_steps = classes // 2, (classes - 1) // 2
@@ -115,12 +123,30 @@
     def at(array, owner):
         return weights.at[array, pl.ds(pl.multiple_of(owner * block, block), block)]
 
-    def along(array, distance):
-        sign = 1 if array % 2 == 0 else -1
-        return lax.rem(z + (sign * distance) % n_sp, n_sp)
+    def along(distance):
+        return lax.rem(z + distance % n_sp, n_sp)
+
+    half_block = block // 2
+    carried = lax.rem(part_at, 2)
+    beside = part_at + 1 - 2 * carried
+
+    def half_at(array, owner, which):
+        start = owner * block + which * half_block
+        return weights.at[array, pl.ds(pl.multiple_of(start, half_block), half_block)]
+
+    def across(array, kind, index, owner, which):
+        ref = half_at(array, owner, which)
+        return pltpu.make_async_remote_copy(
+            src_ref=ref,
+            dst_ref=ref,
+            send_sem=pair_send.at[array, kind, index],
+            recv_sem=pair_recv.at[array, kind, index],
+            device_id={"grp": beside},
+            device_id_type=MESH,
+        )
 
     def hop(array, kind, index, owner, to):
-        ref = at(array, owner)
+        ref = half_at(array, owner, carried)
         return pltpu.make_async_remote_copy(
             src_ref=ref,
             dst_ref=ref,
@@ -133,12 +159,30 @@
     sent_hops = []
 
     def go(array, kind, index, owner, distance):
-        copy = hop(array, kind, index, owner, along(array, distance))
+        copy = hop(array, kind, index, owner, along(distance))
         copy.start()
         sent_hops.append(copy)
 
+    pair_kind = (0, 0, 1, 2, 3)
+
     def come(array, kind, index, owner):
-        hop(array, kind, index, owner, along(array, 1)).wait_recv()
+        hop(array, kind, index, owner, along(1)).wait_recv()
+
+    held_back = [[] for _ in range(2 * LAYERS)]
+
+    def share_out(array, kind, index, owner):
+        copy = across(array, pair_kind[kind], index, owner, carried)
+        if array == 0:
+            copy.start()
+        else:
+            held_back[array].append(copy)
+        sent_hops.append(copy)
+
+    def let_go(arrays):
+        for array in arrays:
+            for copy in held_back[array]:
+                copy.start()
+            held_back[array].clear()
 
     def both(k):
         found = [(k, -STRIDE * k)] if k <= main_steps else []
@@ -149,34 +193,48 @@
     def stride_stage(array, k):
         for index, distance in both(k):
             kind = 0 if distance <= 0 else 1
-            owner = along(array, distance)
+            owner = along(distance)
             if k > 0:
                 come(array, kind, k - 1, owner)
             if (kind == 0) and k < main_steps:
                 go(array, 0, k, owner, STRIDE)
             if (kind == 1 or k == 0) and k < back_steps:
                 go(array, 1, k, owner, -STRIDE)
-            go(array, 2, index, owner, 1)
-            go(array, 4, index, owner, -1)
+            go(array, 2, index, owner, -1)
+            go(array, 4, index, owner, 1)
+            if k > 0:
+                share_out(array, kind, index, owner)
 
     def near_stage(array, k):
         for index, distance in both(k):
-            owner = along(array, distance - 1)
+            owner = along(distance + 1)
             come(array, 2, index, owner)
-            go(array, 3, index, owner, 1)
-
-    def last_stage(array):
+            go(array, 3, index, owner, -1)
+            share_out(array, 2, index, owner)
+
+    def last_stage(array, kind, shift):
         for k in range(main_steps + 1):
             for index, distance in both(k):
-                come(array, 3, index, along(array, distance - 2))
-                come(array, 4, index, along(array, distance + 1))
-
-    def stages(arrays):
+                come(array, kind, index, along(distance + shift))
+                share_out(array, kind, index, along(distance + shift))
+
+    def pair_stage(array):
+        for k in range(main_steps + 1):
+            for index, distance in both(k):
+                for kind, shift in ((0, 0), (1, 1), (2, 2), (3, -1)):
+                    if kind > 0 or k > 0:
+                        across(array, kind, index, along(distance + shift), 1 - carried).wait_recv()
+
+    def stages(array):
         found = []
         for k in range(1, main_steps + 1):
-            found.append([functools.partial(stride_stage, array, k) for array in arrays])
-            found.append([functools.partial(near_stage, array, k - 1) for array in arrays])
-        found.append([functools.partial(near_stage, array, main_steps) for array in arrays])
+            found.append(functools.partial(stride_stage, array, k))
+            if k > 1:
+                found.append(functools.partial(near_stage, array, k - 2))
+        for k in range(max(main_steps - 1, 0), main_steps + 1):
+            found.append(functools.partial(near_stage, array, k))
+        found.append(functools.partial(last_stage, array, 4, -1))
+        found.append(functools.partial(last_stage, array, 3, 2))
         return found
 
     for array in range(2):
@@ -194,7 +252,6 @@
     halo.start()
     for array in range(2, 4):
         loads[array].wait()
-        stride_stage(array, 0)
 
     window = 2 * jnp.where(x == 0, 1, jnp.where(x == 1, 2, jnp.where(x == 2, 4, 8)))
     start = z * rows - HALO + core * share
@@ -207,21 +264,31 @@
     column = lax.broadcasted_iota(jnp.int32, (given, 1), 0) + REACH + start + 1
     scale = 1.0 / jnp.clip(column, 1, window).astype(jnp.float32)
 
-    for stage in stages((0, 1)):
-        for part_of in stage:
-            part_of()
-    later = stages((2, 3))
-
-    def meanwhile(number):
-        for _ in range(number):
+    waves = [stages(array) for array in range(2 * LAYERS)]
+    turns = sorted(
+        (k + LAGS[array], array, k) for array in range(2 * LAYERS) for k in range(len(waves[array]))
+    )
+    done = len(waves[0])
+    for turn, array, k in turns:
+        if turn == 4 and array == 0:
+            stride_stage(2, 0)
+            stride_stage(3, 0)
+        if turn < done:
+            waves[array][k]()
+    later = [waves[array][k] for turn, array, k in turns if turn >= done]
+    polls = list(POLLS)
+
+    def meanwhile(arrays):
+        for _ in range(polls.pop(0) if polls else len(later)):
             if later:
-                for part_of in later.pop(0):
-                    part_of()
+                later.pop(0)()
+        let_go(arrays)
 
     for load in loads[5:]:
         load.wait()
-    last_stage(0)
+    pair_stage(0)
     halo.wait_recv()
+    meanwhile((1,))
 
     sent = []
 
@@ -258,7 +325,7 @@
 
     for layer in range(LAYERS):
         if layer > 0:
-            last_stage(2 * layer)
+            pair_stage(2 * layer)
         order = (xo, xa, xb, x)
 
         def in_weight_of(g):
@@ -292,14 +359,14 @@
 
         f = (first_send, first_recv)
         s = (second_send, second_recv)
-        meanwhile(2)
+        meanwhile(range(2 * LAYERS))
         for half, k, to in ((0, 2, dev_b), (1, 1, dev_a)):
             arrive(first.at[layer, half, 1], f, ((layer, half, 1), (layer, half, 1)))
             second_out[layer, half] = (
                 own[layer, k, half].astype(jnp.float32) + first[layer, half, 1].astype(jnp.float32)
             ).astype(jnp.bfloat16)
             send(second_out.at[layer, half], second.at[layer, half], s, to, ((layer, half), (layer, half)))
-        meanwhile(2)
+        meanwhile(range(2 * LAYERS))
         pieces = []
         for half in range(2):
             arrive(first.at[layer, half, 0], f, ((layer, half, 0), (layer, half, 0)))
@@ -337,14 +404,14 @@
         pass_on(x, 1, dev_b, 3)
         pass_on(x, 0, mate, 4)
         pass_on(x, 1, mate, 5)
-        meanwhile(2)
+        meanwhile(range(2 * LAYERS))
         take_in(core, xb, 0)
         pass_on(xb, 0, dev_a, 6)
         take_in(core, xa, 1)
         pass_on(xa, 1, dev_b, 7)
         pass_on(xb, 0, mate, 8)
         pass_on(xa, 1, mate, 9)
-        meanwhile(2)
+        meanwhile(range(2 * LAYERS))
         take_in(core, xa, 0)
         pass_on(xa, 0, mate, 10)
         take_in(core, xb, 1)
@@ -362,7 +429,7 @@
                 whole, weights[2 * layer + 1], contract, preferred_element_type=jnp.float32
             )
 
-        last_stage(2 * layer + 1)
+        pair_stage(2 * layer + 1)
         summed[pl.ds(mine, given), :] = branch_of(core)
         for g in (x, xb, xa, xo):
             for half in range(2):
@@ -384,7 +451,7 @@
             to = lax.rem(me + step, n_tp)
             send(stat_out.at[layer], stat_in.at[layer, me], q, to, ((layer, step), (layer, me)))
         stat_in[layer, me] = stat_out[layer]
-        meanwhile(len(later))
+        meanwhile(range(2 * LAYERS))
         for step in range(1, n_tp):
             other = lax.rem(me + step, n_tp)
             arrive(stat_in.at[layer, other], q, ((layer, step), (layer, other)))
@@ -448,6 +515,8 @@
             dma((9,)),
             dma((2 * LAYERS, 5, classes)),
             dma((2 * LAYERS, 5, classes)),
+            dma((2 * LAYERS, 4, classes)),
+            dma((2 * LAYERS, 4, classes)),
             dma((2,)),
             dma((LAYERS, GROUPS)),
             dma((LAYERS, GROUPS)),

time: 166 us -> 147 us (0.89)
  Pallas kernels: 163 us -> 145 us
    pallas_call x1, Pallas kernels: 163 us -> 145 us  [per_device(): pl.pallas_call(functools.partial(kernel, n_sp, n_tp), out_shape=jax.Shape...]
where the time goes in v3:
time: 147 us
  Pallas kernels  145 us (99%)
  local copies, waits for them, and re-layouts  2.06 us (1%)
    pallas_call x1, Pallas kernels, per_device(): pl.pallas_call(functools.partial(kernel, n_sp, n_tp), out_shape=jax.Shape...  145 us

profile of v3, /device:TPU:33, one launch (start us, length us, event | category | flops | bytes accessed | tf_op | source)
XLA Modules:
  0.0 147.0 jit_solution(15982664853528809250)
XLA Ops:
  0.0 144.9 %shard_map.73 = bf16[768,512]{1,0:T(8,128)(2,1)} custom-call(bf16[768,512]{1,0:T(8,128)(2,1)} %stream_hbm.1, bf16[2,32,512]{2,1,0:T(8,128)(2,1)} %in_hbm.1, bf16[2,32,512]{2,1,0:T(8,128)(2,1)} %out_hbm.1, bf16[2,4,256,256]{3,2,1,0:T(8,128)(2,1)} %mix_hbm.1, f32[2,1024]{1,0:T(2,128)} %gain_hbm.1, f32[2,512]{1,0:T(2,128)} %norm_gain_hbm.1, f32[2,512]{1,0:T(2,128)} %norm_shift_hbm.1), custom_call_target="tpu_custom_call" | custom-call | tf_op jit(solution)/shard_map/pallas_call | solution.py:492
  144.9 2.1 %copy.9 = bf16[768,512]{1,0:T(8,128)(2,1)} copy(bf16[768,512]{1,0:T(8,128)(2,1)} %shard_map.73) | data formatting | bytes 1572864

commit v4 on v3

--- a/solution.py
+++ b/solution.py
@@ -14,8 +14,7 @@
 HALF = GROUP_WIDTH // 2
 REACH = 16
 STRIDE = 4
-LAGS = (0, 0, 10, 10)
-POLLS = (0, 4, 4, 4, 6, 40)
+POLLS = (2, 4, 4, 4, 4, 40)
 HALO = LAYERS * REACH
 MESH = pl.DeviceIdType.MESH
 
@@ -53,6 +52,7 @@
     load_sem,
     ring_send,
     ring_recv,
+    many_recv,
     pair_send,
     pair_recv,
     halo_sem,
@@ -139,8 +139,8 @@
         return pltpu.make_async_remote_copy(
             src_ref=ref,
             dst_ref=ref,
-            send_sem=pair_send.at[array, kind, index],
-            recv_sem=pair_recv.at[array, kind, index],
+            send_sem=pair_send.at[array],
+            recv_sem=pair_recv.at[array],
             device_id={"grp": beside},
             device_id_type=MESH,
         )
@@ -150,18 +150,18 @@
         return pltpu.make_async_remote_copy(
             src_ref=ref,
             dst_ref=ref,
-            send_sem=ring_send.at[array, kind, index],
-            recv_sem=ring_recv.at[array, kind, index],
+            send_sem=ring_send.at[array],
+            recv_sem=(
+                many_recv.at[array, kind - 3]
+                if kind > 2
+                else ring_recv.at[array, (0, main_steps, main_steps + back_steps)[kind] + index]
+            ),
             device_id={"sp": to},
             device_id_type=MESH,
         )
 
-    sent_hops = []
-
     def go(array, kind, index, owner, distance):
-        copy = hop(array, kind, index, owner, along(distance))
-        copy.start()
-        sent_hops.append(copy)
+        hop(array, kind, index, owner, along(distance)).start()
 
     pair_kind = (0, 0, 1, 2, 3)
 
@@ -176,7 +176,6 @@
             copy.start()
         else:
             held_back[array].append(copy)
-        sent_hops.append(copy)
 
     def let_go(arrays):
         for array in arrays:
@@ -212,18 +211,25 @@
             go(array, 3, index, owner, -1)
             share_out(array, 2, index, owner)
 
+    def wait_many(array, pieces, send_sem, recv_sem):
+        ref = weights.at[array, pl.ds(0, pieces * half_block)]
+        return pltpu.make_async_remote_copy(
+            src_ref=ref,
+            dst_ref=ref,
+            send_sem=send_sem,
+            recv_sem=recv_sem,
+            device_id={"grp": beside},
+            device_id_type=MESH,
+        )
+
     def last_stage(array, kind, shift):
+        wait_many(array, classes, ring_send.at[array], many_recv.at[array, kind - 3]).wait_recv()
         for k in range(main_steps + 1):
             for index, distance in both(k):
-                come(array, kind, index, along(distance + shift))
                 share_out(array, kind, index, along(distance + shift))
 
     def pair_stage(array):
-        for k in range(main_steps + 1):
-            for index, distance in both(k):
-                for kind, shift in ((0, 0), (1, 1), (2, 2), (3, -1)):
-                    if kind > 0 or k > 0:
-                        across(array, kind, index, along(distance + shift), 1 - carried).wait_recv()
+        wait_many(array, n_sp - 1, pair_send.at[array], pair_recv.at[array]).wait_recv()
 
     def stages(array):
         found = []
@@ -266,7 +272,9 @@
 
     waves = [stages(array) for array in range(2 * LAYERS)]
     turns = sorted(
-        (k + LAGS[array], array, k) for array in range(2 * LAYERS) for k in range(len(waves[array]))
+        (k if array < 2 else 8 if k == 0 else len(waves[0]) + k, array, k)
+        for array in range(2 * LAYERS)
+        for k in range(len(waves[array]))
     )
     done = len(waves[0])
     for turn, array, k in turns:
@@ -290,29 +298,28 @@
     halo.wait_recv()
     meanwhile((1,))
 
-    sent = []
-
-    def send(src, dst, sems, to, index):
-        copy = pltpu.make_async_remote_copy(
+    def send(src, dst, sems, to, layer, index):
+        pltpu.make_async_remote_copy(
             src_ref=src,
             dst_ref=dst,
-            send_sem=sems[0].at[index[0]],
-            recv_sem=sems[1].at[index[1]],
+            send_sem=sems[0].at[layer],
+            recv_sem=sems[1].at[index],
             device_id={"tp": to},
             device_id_type=MESH,
-        )
-        copy.start()
-        sent.append(copy)
-
-    def arrive(dst, sems, index):
-        pltpu.make_async_remote_copy(
-            src_ref=dst,
-            dst_ref=dst,
-            send_sem=sems[0].at[index[0]],
-            recv_sem=sems[1].at[index[1]],
+        ).start()
+
+    def waiting(ref, sems, layer, index):
+        return pltpu.make_async_remote_copy(
+            src_ref=ref,
+            dst_ref=ref,
+            send_sem=sems[0].at[layer],
+            recv_sem=sems[1].at[index],
             device_id={"tp": mate},
             device_id_type=MESH,
-        ).wait_recv()
+        )
+
+    def arrive(ref, sems, layer, index):
+        waiting(ref, sems, layer, index).wait_recv()
 
     contract_cols = (((1,), (1,)), ((), ()))
     contract = (((1,), (0,)), ((), ()))
@@ -323,6 +330,9 @@
         jnp.int32, (rblock, 128), 1
     )
 
+    def piece(side, g, half):
+        return (side * GROUPS + g) * 2 + half
+
     for layer in range(LAYERS):
         if layer > 0:
             pair_stage(2 * layer)
@@ -331,46 +341,53 @@
         def in_weight_of(g):
             return weights[2 * layer, pl.ds(pl.multiple_of(g * GROUP_WIDTH, GROUP_WIDTH), GROUP_WIDTH)]
 
-        for k, g in enumerate(order):
-            product = lax.dot_general(
-                cur[pl.ds(mates, taken)], in_weight_of(g), contract_cols,
-                preferred_element_type=jnp.float32,
-            )
+        p = (part_send, part_recv)
+        f = (first_send, first_recv)
+        s = (second_send, second_recv)
+        c = (gath_send, gath_recv)
+        q = (stat_send, stat_recv)
+
+        def product_of(k):
+            of_g = in_weight_of(order[k])
+            product = lax.dot_general(cur[...], of_g, contract_cols, preferred_element_type=jnp.float32)
             part[layer, k] = product.astype(jnp.bfloat16)
-            send(part.at[layer, k], peer.at[layer, k], (part_send, part_recv), mate,
-                 ((layer, k), (layer, k)))
-        for k, g in enumerate(order):
-            product = lax.dot_general(
-                cur[pl.ds(mine, taken)], in_weight_of(g), contract_cols,
-                preferred_element_type=jnp.float32,
-            )
-            arrive(peer.at[layer, k], (part_send, part_recv), ((layer, k), (layer, k)))
-            total = (product + peer[layer, k].astype(jnp.float32)).astype(jnp.bfloat16)
+            send(part.at[layer, k, pl.ds(mates, taken)], peer.at[layer, k], p, mate, layer, (layer, k))
+
+        def reduce_pair(k):
+            arrive(peer.at[layer, k], p, layer, (layer, k))
+            total = (
+                part[layer, k, pl.ds(mine, taken)].astype(jnp.float32) + peer[layer, k].astype(jnp.float32)
+            ).astype(jnp.bfloat16)
             own[layer, k, 0] = total[:, :HALF]
             own[layer, k, 1] = total[:, HALF:]
-            f = (first_send, first_recv)
             if k == 0:
-                send(own.at[layer, 0, 0], first.at[layer, 0, 1], f, dev_a, ((layer, 0, 1), (layer, 0, 1)))
-                send(own.at[layer, 0, 1], first.at[layer, 1, 1], f, dev_b, ((layer, 1, 1), (layer, 1, 1)))
+                send(own.at[layer, 0, 0], first.at[layer, 0, 1], f, dev_a, layer, (layer, 0, 1))
+                send(own.at[layer, 0, 1], first.at[layer, 1, 1], f, dev_b, layer, (layer, 1, 1))
             if k == 1:
-                send(own.at[layer, 1, 0], first.at[layer, 0, 0], f, dev_a, ((layer, 0, 0), (layer, 0, 0)))
+                send(own.at[layer, 1, 0], first.at[layer, 0, 0], f, dev_a, layer, (layer, 0, 0))
             if k == 2:
-                send(own.at[layer, 2, 1], first.at[layer, 1, 0], f, dev_b, ((layer, 1, 0), (layer, 1, 0)))
-
-        f = (first_send, first_recv)
-        s = (second_send, second_recv)
+                send(own.at[layer, 2, 1], first.at[layer, 1, 0], f, dev_b, layer, (layer, 1, 0))
+
+        product_of(0)
+        product_of(1)
+        product_of(2)
+        reduce_pair(0)
+        product_of(3)
+        reduce_pair(1)
+        reduce_pair(2)
+        reduce_pair(3)
         meanwhile(range(2 * LAYERS))
         for half, k, to in ((0, 2, dev_b), (1, 1, dev_a)):
-            arrive(first.at[layer, half, 1], f, ((layer, half, 1), (layer, half, 1)))
+            arrive(first.at[layer, half, 1], f, layer, (layer, half, 1))
             second_out[layer, half] = (
                 own[layer, k, half].astype(jnp.float32) + first[layer, half, 1].astype(jnp.float32)
             ).astype(jnp.bfloat16)
-            send(second_out.at[layer, half], second.at[layer, half], s, to, ((layer, half), (layer, half)))
+            send(second_out.at[layer, half], second.at[layer, half], s, to, layer, (layer, half))
         meanwhile(range(2 * LAYERS))
         pieces = []
         for half in range(2):
-            arrive(first.at[layer, half, 0], f, ((layer, half, 0), (layer, half, 0)))
-            arrive(second.at[layer, half], s, ((layer, half), (layer, half)))
+            arrive(first.at[layer, half, 0], f, layer, (layer, half, 0))
+            arrive(second.at[layer, half], s, layer, (layer, half))
             pieces.append(
                 (
                     own[layer, 3, half].astype(jnp.float32)
@@ -387,43 +404,43 @@
             of_g = gain_ref[pl.ds(layer, 1), pl.ds(g * GROUP_WIDTH, GROUP_WIDTH)]
             gains = jnp.where(x == g, of_g, gains)
         scaled = (mixed * gains).astype(jnp.bfloat16)
-        gath[layer, core, x, 0] = scaled[:, :HALF]
-        gath[layer, core, x, 1] = scaled[:, HALF:]
-
-        def pass_on(g, half, to, slot):
-            ref = gath.at[layer, core, g, half]
-            send(ref, ref, (gath_send, gath_recv), to, ((layer, slot), (layer, core, g, half)))
-
-        def take_in(side, g, half):
-            arrive(gath.at[layer, side, g, half], (gath_send, gath_recv),
-                   ((layer, 0), (layer, side, g, half)))
-
-        pass_on(x, 0, dev_b, 0)
-        pass_on(x, 1, dev_a, 1)
-        pass_on(x, 0, dev_a, 2)
-        pass_on(x, 1, dev_b, 3)
-        pass_on(x, 0, mate, 4)
-        pass_on(x, 1, mate, 5)
+        gath[layer, piece(core, x, 0)] = scaled[:, :HALF]
+        gath[layer, piece(core, x, 1)] = scaled[:, HALF:]
+
+        def pass_on(g, half, to):
+            ref = gath.at[layer, piece(core, g, half)]
+            index = 2 * GROUPS if to is mate else 2 * g + half
+            send(ref, ref, c, to, layer, (layer, index))
+
+        def take_in(g, half):
+            arrive(gath.at[layer, piece(core, g, half)], c, layer, (layer, 2 * g + half))
+
+        pass_on(x, 0, dev_b)
+        pass_on(x, 1, dev_a)
+        pass_on(x, 0, dev_a)
+        pass_on(x, 1, dev_b)
+        pass_on(x, 0, mate)
+        pass_on(x, 1, mate)
         meanwhile(range(2 * LAYERS))
-        take_in(core, xb, 0)
-        pass_on(xb, 0, dev_a, 6)
-        take_in(core, xa, 1)
-        pass_on(xa, 1, dev_b, 7)
-        pass_on(xb, 0, mate, 8)
-        pass_on(xa, 1, mate, 9)
+        take_in(xb, 0)
+        pass_on(xb, 0, dev_a)
+        take_in(xa, 1)
+        pass_on(xa, 1, dev_b)
+        pass_on(xb, 0, mate)
+        pass_on(xa, 1, mate)
         meanwhile(range(2 * LAYERS))
-        take_in(core, xa, 0)
-        pass_on(xa, 0, mate, 10)
-        take_in(core, xb, 1)
-        pass_on(xb, 1, mate, 11)
-        take_in(core, xo, 0)
-        pass_on(xo, 0, mate, 12)
-        take_in(core, xo, 1)
-        pass_on(xo, 1, mate, 13)
+        take_in(xa, 0)
+        pass_on(xa, 0, mate)
+        take_in(xb, 1)
+        pass_on(xb, 1, mate)
+        take_in(xo, 0)
+        pass_on(xo, 0, mate)
+        take_in(xo, 1)
+        pass_on(xo, 1, mate)
 
         def branch_of(side):
             whole = jnp.concatenate(
-                [gath[layer, side, g, half] for g in range(GROUPS) for half in range(2)], axis=1
+                [gath[layer, piece(side, g, half)] for g in range(GROUPS) for half in range(2)], axis=1
             )
             return lax.dot_general(
                 whole, weights[2 * layer + 1], contract, preferred_element_type=jnp.float32
@@ -431,9 +448,7 @@
 
         pair_stage(2 * layer + 1)
         summed[pl.ds(mine, given), :] = branch_of(core)
-        for g in (x, xb, xa, xo):
-            for half in range(2):
-                take_in(1 - core, g, half)
+        arrive(gath.at[layer, pl.ds(piece(1 - core, 0, 0), 2 * GROUPS)], c, layer, (layer, 2 * GROUPS))
         summed[pl.ds(mates, given), :] = branch_of(1 - core)
 
         stat_out[layer] = jnp.zeros((16, 128), jnp.float32)
@@ -446,15 +461,12 @@
                 stat_out[layer, pl.ds(at_row, 1), :] = jnp.sum(
                     jnp.where(eye, total, 0.0), axis=0, keepdims=True
                 )
-        q = (stat_send, stat_recv)
         for step in range(1, n_tp):
             to = lax.rem(me + step, n_tp)
-            send(stat_out.at[layer], stat_in.at[layer, me], q, to, ((layer, step), (layer, me)))
+            send(stat_out.at[layer], stat_in.at[layer, me], q, to, layer, layer)
         stat_in[layer, me] = stat_out[layer]
         meanwhile(range(2 * LAYERS))
-        for step in range(1, n_tp):
-            other = lax.rem(me + step, n_tp)
-            arrive(stat_in.at[layer, other], q, ((layer, step), (layer, other)))
+        arrive(stat_in.at[layer, pl.ds(0, n_tp - 1)], q, layer, layer)
         stats = stat_in[layer, 0]
         for k in range(1, n_tp):
             stats = stats + stat_in[layer, k]
@@ -477,8 +489,15 @@
             else:
                 out_ref[pl.ds(b * rblock - REACH, rblock), :] = value.astype(jnp.bfloat16)
 
-    for copy in sent + sent_hops:
-        copy.wait_send()
+    for layer in range(LAYERS):
+        waiting(peer.at[layer], p, layer, (layer, 0)).wait_send()
+        waiting(first.at[layer], f, layer, (layer, 0, 0)).wait_send()
+        waiting(second.at[layer], s, layer, (layer, 0)).wait_send()
+        waiting(gath.at[layer, pl.ds(0, 4 * GROUPS - 2)], c, layer, (layer, 0)).wait_send()
+        waiting(stat_in.at[layer, pl.ds(0, n_tp - 1)], q, layer, layer).wait_send()
+    for array in range(2 * LAYERS):
+        wait_many(array, n_sp - 1, ring_send.at[array], pair_recv.at[array]).wait_send()
+        wait_many(array, n_sp - 1, pair_send.at[array], pair_recv.at[array]).wait_send()
 
 
 def per_device(n_sp, n_tp, stream, in_weight, out_weight, group_mix, pool_gain, norm_gain, norm_shift):
@@ -502,32 +521,33 @@
             pltpu.VMEM((2 * LAYERS, pool, cols), bf),
             pltpu.VMEM((rows + HALO, cols), bf),
             pltpu.VMEM((given, taken), bf),
-            pltpu.VMEM((LAYERS, GROUPS, taken, GROUP_WIDTH), bf),
+            pltpu.VMEM((LAYERS, GROUPS, rows + HALO, GROUP_WIDTH), bf),
             pltpu.VMEM((LAYERS, GROUPS, taken, GROUP_WIDTH), bf),
             pltpu.VMEM((LAYERS, GROUPS, 2, taken, HALF), bf),
             pltpu.VMEM((LAYERS, 2, 2, taken, HALF), bf),
             pltpu.VMEM((LAYERS, 2, taken, HALF), bf),
             pltpu.VMEM((LAYERS, 2, taken, HALF), bf),
-            pltpu.VMEM((LAYERS, 2, GROUPS, 2, given, HALF), bf),
+            pltpu.VMEM((LAYERS, 4 * GROUPS, given, HALF), bf),
             pltpu.VMEM((rows + REACH, cols), f32),
             pltpu.VMEM((LAYERS, 16, 128), f32),
             pltpu.VMEM((LAYERS, n_tp, 16, 128), f32),
             dma((9,)),
-            dma((2 * LAYERS, 5, classes)),
-            dma((2 * LAYERS, 5, classes)),
-            dma((2 * LAYERS, 4, classes)),
-            dma((2 * LAYERS, 4, classes)),
+            dma((2 * LAYERS,)),
+            dma((2 * LAYERS, 2 * classes)),
+            dma((2 * LAYERS, 2)),
+            dma((2 * LAYERS,)),
+            dma((2 * LAYERS,)),
             dma((2,)),
+            dma((LAYERS,)),
             dma((LAYERS, GROUPS)),
-            dma((LAYERS, GROUPS)),
+            dma((LAYERS,)),
             dma((LAYERS, 2, 2)),
-            dma((LAYERS, 2, 2)),
+            dma((LAYERS,)),
             dma((LAYERS, 2)),
-            dma((LAYERS, 2)),
-            dma((LAYERS, 14)),
-            dma((LAYERS, 2, GROUPS, 2)),
-            dma((LAYERS, n_tp)),
-            dma((LAYERS, n_tp)),
+            dma((LAYERS,)),
+            dma((LAYERS, 2 * GROUPS + 1)),
+            dma((LAYERS,)),
+            dma((LAYERS,)),
         ],
         compiler_params=pltpu.CompilerParams(
             collective_id=0, has_side_effects=True, vmem_limit_bytes=60 * 1024 * 1024

time: 147 us -> 141 us (0.959)
  Pallas kernels: 145 us -> 139 us
    pallas_call x1, Pallas kernels: 145 us -> 139 us  [per_device(): pl.pallas_call(functools.partial(kernel, n_sp, n_tp), out_shape=jax.Shape...]
where the time goes in v4:
time: 141 us
  Pallas kernels  139 us (99%)
  local copies, waits for them, and re-layouts  2.06 us (1%)
    pallas_call x1, Pallas kernels, per_device(): pl.pallas_call(functools.partial(kernel, n_sp, n_tp), out_shape=jax.Shape...  139 us

profile of v4, /device:TPU:33, one launch (start us, length us, event | category | flops | bytes accessed | tf_op | source)
XLA Modules:
  0.0 140.8 jit_solution(15891679932610545517)
XLA Ops:
  0.0 138.7 %shard_map.73 = bf16[768,512]{1,0:T(8,128)(2,1)} custom-call(bf16[768,512]{1,0:T(8,128)(2,1)} %stream_hbm.1, bf16[2,32,512]{2,1,0:T(8,128)(2,1)} %in_hbm.1, bf16[2,32,512]{2,1,0:T(8,128)(2,1)} %out_hbm.1, bf16[2,4,256,256]{3,2,1,0:T(8,128)(2,1)} %mix_hbm.1, f32[2,1024]{1,0:T(2,128)} %gain_hbm.1, f32[2,512]{1,0:T(2,128)} %norm_gain_hbm.1, f32[2,512]{1,0:T(2,128)} %norm_shift_hbm.1), custom_call_target="tpu_custom_call" | custom-call | tf_op jit(solution)/shard_map/pallas_call | solution.py:511
  138.7 2.1 %copy.9 = bf16[768,512]{1,0:T(8,128)(2,1)} copy(bf16[768,512]{1,0:T(8,128)(2,1)} %shard_map.73) | data formatting | bytes 1572864
